TPU v7x, 32 devices: a whole 2x2x4 slice. The times are simulated.
32 devices in a mesh: sp: 16 (over z, y, x), tp: 2 (over core).
Axes of the slice: x: 2, y: 2, z: 4, core: 2. Of those that a mesh axis runs over, the one named last changes fastest.
Arguments:
- tokens: bfloat16 [4096, 2048], P(('sp', 'tp')), may hold values from -6 to 6
- mix_gain: float32 [2048], replicated, may hold values from 0.1 to 1.9
- query_proj: bfloat16 [2048, 1536], P(None, 'tp'), may hold values from -4 to 4
- compressed_projection: bfloat16 [2048, 256], replicated, may hold values from -0.125 to 0.125
- compressed_norm_gain: float32 [256], replicated, may hold values from 0.1 to 1.9
- rope_proj: bfloat16 [2048, 64], replicated, may hold values from -0.125 to 0.125
- key_up: bfloat16 [256, 1024], P(None, 'tp'), may hold values from -4 to 4
- value_up_weight: bfloat16 [256, 1024], P(None, 'tp'), may hold values from -0.375 to 0.375
- scan_input: bfloat16 [2048, 2048], P('sp', 'tp'), may hold values from -0.125 to 0.125
- scan_gate: bfloat16 [2048, 2048], P('sp', 'tp'), may hold values from -0.125 to 0.125
- scan_write: bfloat16 [2048, 1024], P('sp', 'tp'), may hold values from -0.125 to 0.125
- scan_read: bfloat16 [2048, 1024], P('sp', 'tp'), may hold values from -0.125 to 0.125
- step_proj: bfloat16 [2048, 32], replicated, may hold values from -0.125 to 0.125
- conv_input: bfloat16 [4, 2048], P(None, 'tp'), may hold values from -3 to 3
- conv_write: bfloat16 [4, 1024], P(None, 'tp'), may hold values from -3 to 3
- conv_read: bfloat16 [4, 1024], P(None, 'tp'), may hold values from -3 to 3
- decay_log: float32 [32], P('tp'), may hold values from -16 to -2.8
- decay_offset: float32 [4096, 32], P('sp', 'tp'), may hold values from -2.2 to 0
- skip_gain: float32 [32], P('tp'), may hold values from 0.1 to 1.9
- group_gain: float32 [2048], P('tp'), may hold values from 0.1 to 1.9
Outputs:
- attended: bfloat16 [4096, 1024], P('sp', 'tp')
- scanned: bfloat16 [4096, 2048], P('sp', 'tp')
All inputs are finite; a program needn't handle non-finite values.
Results may differ from a plain program's by a relative error of at most 0.017.
The roundings to bfloat16 on the way count: a program that leaves them out, or rounds other values in their place, can miss the bound.
Values may be sent and summed in bfloat16 or wider, within the bound.
A program may use at most 128 MiB of HBM per device.

v0:
```python
import jax
import jax.numpy as jnp
from jax import lax
from jax.sharding import PartitionSpec as P

UNROTATED_WIDTH = 128
ROPE = 64
VALUE_WIDTH = 128
SSM_DIM = 64
SSM_STATE = 128
eps = 1e-06
theta = 10000.0
floor_score = -1e30


def from_behind(value, axis, steps):
    count = lax.axis_size(axis)
    initial, last = (max(0, -steps), min(count, count - steps))
    return lax.ppermute(value, axis, [(source, source + steps) for source in range(initial, last)])


def rms_scale(values, gain):
    wide = values.astype(jnp.float32)
    return wide * lax.rsqrt(jnp.mean(wide * wide, axis=-1, keepdims=True) + eps) * gain


def rotate(values, positions):
    half = values.shape[-1] // 2
    freqs = theta ** (-jnp.arange(half, dtype=jnp.float32) * 2.0 / values.shape[-1])
    angle = positions.astype(jnp.float32)[:, None] * freqs[None, :]
    cosine = jnp.cos(angle)
    sine = jnp.sin(angle)
    if values.ndim == 3:
        cosine = cosine[:, None, :]
        sine = sine[:, None, :]
    first = values[..., :half]
    second = values[..., half:]
    return jnp.concatenate(
        [first * cosine - second * sine, second * cosine + first * sine], axis=-1
    )


def short_conv(values, edge, taps):
    span = taps.shape[0]
    length = values.shape[0]
    padded = jnp.concatenate([edge, values], axis=0).astype(jnp.float32)
    result = jnp.zeros(values.shape, jnp.float32)
    for index in range(span):
        result = result + taps[index].astype(jnp.float32)[None, :] * padded[index : index + length]
    return jax.nn.silu(result).astype(jnp.bfloat16)


def local_scan(heads, steps, decays, writes, reads):
    length = decays.shape[-1]
    running = jnp.einsum(
        "grs,ls->grl",
        decays,
        jnp.tril(jnp.ones((length, length), jnp.float32)),
        precision=lax.Precision.HIGHEST,
    )
    causal = jnp.tril(jnp.ones((length, length), dtype=bool))
    spread = jnp.where(causal, running[..., :, None] - running[..., None, :], -jnp.inf)
    inner = jnp.einsum("gln,gsn->gls", reads, writes, preferred_element_type=jnp.float32)
    mixing = inner[:, None] * jnp.exp(spread) * steps[:, :, None, :]
    within = jnp.einsum(
        "grls,grsp->grlp", mixing.astype(jnp.bfloat16), heads, preferred_element_type=jnp.float32
    )
    to_end = jnp.exp(running[..., -1:] - running) * steps
    weighted = (heads.astype(jnp.float32) * to_end[..., None]).astype(jnp.bfloat16)
    state = jnp.einsum("grsp,gsn->grpn", weighted, writes, preferred_element_type=jnp.float32)
    return (running, state, within)


def state_before(state, total, axis):
    groups, per_group, dim, entries = state.shape
    count = groups * per_group
    flat = state.reshape(count * dim, entries).astype(jnp.bfloat16)
    high = total.reshape(count).astype(jnp.bfloat16)
    low = (total.reshape(count) - high.astype(jnp.float32)).astype(jnp.bfloat16)
    tail = jnp.zeros((16, entries), jnp.bfloat16)
    tail = tail.at[0, :count].set(high).at[1, :count].set(low)
    everything = lax.all_gather(jnp.concatenate([flat, tail], axis=0), axis)
    here = lax.axis_index(axis)
    devices = everything.shape[0]
    states = everything[:, : count * dim].reshape(devices, count, dim, entries)
    totals = everything[:, count * dim, :count].astype(jnp.float32) + everything[
        :, count * dim + 1, :count
    ].astype(jnp.float32)
    index = jnp.arange(devices)
    between = (index[None, :] > index[:, None]) & (index[None, :] < here)
    path = jnp.sum(jnp.where(between[:, :, None], totals[None], 0.0), axis=1)
    factor = jnp.where((index < here)[:, None], jnp.exp(path), 0.0)
    before = jnp.sum(states.astype(jnp.float32) * factor[:, :, None, None], axis=0)
    return before.reshape(state.shape)


def gated_norm(mixed, gate, gain):
    length = mixed.shape[0]
    groups = mixed.shape[1]
    flat = mixed.reshape(length, groups, -1)
    gated = flat * jax.nn.silu(gate.astype(jnp.float32)).reshape(length, groups, -1)
    scaled = gated * lax.rsqrt(jnp.mean(gated * gated, axis=-1, keepdims=True) + eps)
    return (scaled * gain.reshape(groups, -1)[None]).reshape(length, -1).astype(jnp.bfloat16)


def attend_piece(
    carry,
    query_plain,
    query_turned,
    query_positions,
    latent,
    key_turned,
    key_positions,
    key_up,
    value_up_weight,
):
    highest, total, summed = carry
    heads = query_plain.shape[1]
    count = latent.shape[0]
    key_plain = (
        jnp.dot(latent, key_up, preferred_element_type=jnp.float32)
        .astype(jnp.bfloat16)
        .reshape(count, heads, -1)
    )
    values = (
        jnp.dot(latent, value_up_weight, preferred_element_type=jnp.float32)
        .astype(jnp.bfloat16)
        .reshape(count, heads, -1)
    )
    scale = (query_plain.shape[-1] + query_turned.shape[-1]) ** (-0.5)
    query_whole = jnp.concatenate([query_plain, query_turned], axis=-1)
    shared_turned = jnp.broadcast_to(key_turned[:, None, :], (count, heads, key_turned.shape[-1]))
    key_whole = jnp.concatenate([key_plain, shared_turned], axis=-1)
    scores = (
        jnp.einsum("qhd,khd->hqk", query_whole, key_whole, preferred_element_type=jnp.float32)
        * scale
    )
    scores = jnp.where(
        key_positions[None, None, :] <= query_positions[None, :, None], scores, -jnp.inf
    )
    new_highest = jnp.maximum(highest, jnp.max(scores, axis=-1))
    weights = jnp.exp(scores - new_highest[..., None])
    total = jnp.sum(weights, axis=-1)
    summed = jnp.einsum(
        "hqk,khd->hqd", weights.astype(jnp.bfloat16), values, preferred_element_type=jnp.float32
    )
    return (new_highest, total, summed)


def shards(
    tokens,
    mix_gain,
    query_proj,
    compressed_projection,
    compressed_norm_gain,
    rope_proj,
    key_up,
    value_up_weight,
    scan_input,
    scan_gate,
    scan_write,
    scan_read,
    step_proj,
    conv_input,
    conv_write,
    conv_read,
    decay_log,
    decay_offset,
    skip_gain,
    group_gain,
):
    own_normed = rms_scale(tokens, mix_gain).astype(jnp.bfloat16)
    rows = lax.all_gather(own_normed, "tp", axis=0, tiled=True)
    length = rows.shape[0]
    width = tokens.shape[1]
    sp_index = lax.axis_index("sp")
    positions = sp_index * length + jnp.arange(length, dtype=jnp.int32)
    heads = key_up.shape[1] // UNROTATED_WIDTH
    local_heads = decay_log.shape[0]
    latent_width = compressed_projection.shape[1]
    small = jnp.dot(
        rows,
        jnp.concatenate([compressed_projection, rope_proj, step_proj], axis=1),
        preferred_element_type=jnp.float32,
    )
    latent = rms_scale(small[:, :latent_width], compressed_norm_gain).astype(jnp.bfloat16)
    key_turned = rotate(small[:, latent_width : latent_width + ROPE], positions).astype(
        jnp.bfloat16
    )
    step_all = small[:, latent_width + ROPE :]
    edge_rows = from_behind(rows[length - 8 :], "sp", 1)
    keys = jnp.concatenate([latent, key_turned], axis=1)
    depth = scan_input.shape[0]
    packed = jnp.concatenate(
        [scan_input, scan_gate, scan_write, scan_read, keys.reshape(depth, -1)], axis=1
    )
    everything = lax.all_gather(packed, "sp", axis=0, tiled=True)
    widths = [w.shape[1] for w in (scan_input, scan_gate, scan_write, scan_read)]
    scan_width = sum(widths)
    all_keys = everything[:, scan_width:].reshape(-1, latent_width + ROPE)
    projected = jnp.dot(
        jnp.concatenate([edge_rows, rows], axis=0),
        everything[:, :scan_width],
        preferred_element_type=jnp.float32,
    ).astype(jnp.bfloat16)
    edge, projected = (projected[:8], projected[8:])
    gate = projected[:, widths[0] : widths[0] + widths[1]]
    span = conv_input.shape[0] - 1

    def convolved(start, size, taps):
        return short_conv(
            projected[:, start : start + size], edge[8 - span :, start : start + size], taps
        )

    head_conv = convolved(0, widths[0], conv_input)
    writes = convolved(widths[0] + widths[1], widths[2], conv_write)
    reads = convolved(widths[0] + widths[1] + widths[2], widths[3], conv_read)
    step_size = jax.nn.softplus(
        lax.dynamic_slice_in_dim(step_all, lax.axis_index("tp") * local_heads, local_heads, 1)
    )
    groups = scan_write.shape[1] // SSM_STATE
    per_group = local_heads // groups
    log_decay = -jnp.exp(decay_log)[None, :] * step_size + decay_offset
    head_values = jnp.transpose(head_conv.reshape(length, groups, per_group, SSM_DIM), (1, 2, 0, 3))
    step_values = step_size.T.reshape(groups, per_group, length)
    decay_values = log_decay.T.reshape(groups, per_group, length)
    write_values = jnp.transpose(writes.reshape(length, groups, SSM_STATE), (1, 0, 2))
    read_values = jnp.transpose(reads.reshape(length, groups, SSM_STATE), (1, 0, 2))
    running, final_state, mixed = local_scan(
        head_values, step_values, decay_values, write_values, read_values
    )
    incoming = state_before(final_state, running[..., -1], "sp")
    carried = jnp.einsum(
        "gln,grpn->grlp",
        read_values,
        incoming.astype(jnp.bfloat16),
        preferred_element_type=jnp.float32,
    )
    mixed = (
        mixed
        + carried * jnp.exp(running)[..., None]
        + skip_gain.reshape(groups, per_group)[:, :, None, None] * head_values.astype(jnp.float32)
    )
    scanned = gated_norm(jnp.transpose(mixed, (2, 0, 1, 3)), gate, group_gain)
    query = jnp.dot(rows, query_proj, preferred_element_type=jnp.float32).astype(jnp.bfloat16)
    query = query.reshape(length, heads, UNROTATED_WIDTH + ROPE)
    query_plain = query[:, :, :UNROTATED_WIDTH]
    query_turned = rotate(query[:, :, UNROTATED_WIDTH:].astype(jnp.float32), positions).astype(
        jnp.bfloat16
    )
    initial = (
        jnp.full((heads, length), floor_score, jnp.float32),
        jnp.zeros((heads, length), jnp.float32),
        jnp.zeros((heads, length, VALUE_WIDTH), jnp.float32),
    )
    key_positions = jnp.arange(all_keys.shape[0], dtype=jnp.int32)
    _, total, summed = attend_piece(
        initial,
        query_plain,
        query_turned,
        positions,
        all_keys[:, :latent_width],
        all_keys[:, latent_width:],
        key_positions,
        key_up,
        value_up_weight,
    )
    attended = jnp.transpose((summed / total[..., None]).astype(jnp.bfloat16), (1, 0, 2)).reshape(
        length, heads * VALUE_WIDTH
    )
    return (attended, scanned)


def solution(mesh):
    in_specs = (
        P(("sp", "tp"), None),
        P(),
        P(None, "tp"),
        P(),
        P(),
        P(),
        P(None, "tp"),
        P(None, "tp"),
        P("sp", "tp"),
        P("sp", "tp"),
        P("sp", "tp"),
        P("sp", "tp"),
        P(),
        P(None, "tp"),
        P(None, "tp"),
        P(None, "tp"),
        P("tp"),
        P("sp", "tp"),
        P("tp"),
        P("tp"),
    )
    out_specs = (P("sp", "tp"), P("sp", "tp"))
    return jax.shard_map(shards, mesh=mesh, in_specs=in_specs, out_specs=out_specs, check_vma=False)
```

profile of v0, /device:TPU:0, one launch (start us, length us, event | category | flops | bytes accessed | tf_op | source)
XLA Modules:
  0.0 320.8 jit_solution(13129641332036617341)
XLA Ops:
  7.2 1.4 fusion.40
  8.6 2.0 fusion.42
  10.7 2.0 copy.58
  12.7 1.9 copy.59
  14.6 0.6 multiply_power_fusion
  15.2 0.6 fusion.81
  15.8 1.7 constant_dynamic-update-slice_fusion.4
  17.4 0.7 constant_dynamic-update-slice_fusion.3
  18.2 0.7 constant_dynamic-update-slice_fusion.2
  18.8 1.6 constant_dynamic-update-slice_fusion.1
  20.5 2.1 all-gather.5.cloned.1.call-done
  22.6 3.2 %fusion.24 = f32[256,352]{0,1:T(8,128)S(1)} fusion(bf16[256,2048]{1,0:T(8,128)(2,1)} %all-gather.5.cloned.1.call-done, bf16[2048,32]{1,0:T(8,128)(2,1)} %copy.59, bf16[2048,64]{1,0:T(8,128)(2,1)} %copy.58, bf16[2048,256]{1,0:T(8,128)(2,1)} %param.27), kind=kOutput, calls=%fused_computation.28 | convolution fusion | flops 373424128 | bytes 2850816 | tf_op jit(solution)/shard_map/dot_general | solution.py:181
  25.9 0.8 subtract_convert_fusion.1
  26.7 0.8 multiply_convert_fusion.10
  27.9 0.7 constant_dynamic-update-slice_fusion
  28.7 0.7 iota_compare_fusion.1
  29.3 0.7 exponential_negate_fusion
  30.1 0.8 slice.235
  30.8 3.6 %collective-permute-start = (bf16[8,2048]{1,0:T(8,128)(2,1)S(1)}, bf16[8,2048]{1,0:T(8,128)(2,1)S(1)}, u32[]{:S(2)}, u32[]{:S(2)}) collective-permute-start(bf16[8,2048]{1,0:T(8,128)(2,1)S(1)} %slice.235), channel_id=1, source_target_pairs={{0,2},{2,4},{4,6},{6,8},{8,10},{10,12},{12,14},{14,16},{16,18},{18... | collective-permute-start | bytes 98312 | tf_op jit(solution)/shard_map/ppermute | solution.py:19
  34.5 0.8 add_bitcast_fusion
  35.3 0.3 fusion.68
  36.0 0.3 scatter.9
  36.4 169.7 %all-gather.7.cloned.1.call-done = bf16[2048,3712]{1,0:T(8,128)(2,1)} async-done(((bf16[128,3712]{1,0:T(8,128)(2,1)}), bf16[2048,3712]{1,0:T(8,128)(2,1)}) %all-gather.7.cloned.1.call-update) | async-done | bytes 15204368 | tf_op jit(solution)/shard_map/all_gather | solution.py:197
  206.1 8.4 %fusion.12 = bf16[264,3072]{1,0:T(8,128)(2,1)S(1)} fusion(bf16[2048,3712]{1,0:T(8,128)(2,1)} %all-gather.7.cloned.1.call-done, bf16[256,2048]{1,0:T(8,128)(2,1)} %all-gather.5.cloned.1.call-done, bf16[8,2048]{1,0:T(8,128)(2,1)S(1)} %collective-permute-done), kind=kOutput, calls=%fused_computation.18 | convolution fusion | flops 3324862464 | bytes 15286272 | tf_op jit(solution)/shard_map/dot_general | solution.py:201
  214.5 1.3 slice_convert_fusion.2
  215.9 0.2 copy-done.6
  216.2 1.4 multiply_convert_fusion.6
  217.7 2.1 copy.64
  219.7 4.1 %fusion.71 = (bf16[32,4,8,128]{3,2,1,0:T(8,128)(2,1)}, bf16[32,4,8,128]{3,2,1,0:T(8,128)(2,1)S(1)}) fusion(f32[259,512]{1,0:T(8,128)} %get-tuple-element.36, f32[512]{0:T(512)S(1)} %bitcast.121, f32[512]{0:T(512)S(1)} %bitcast.122, f32[512]{0:T(512)S(1)} %bitcast.120, f32[512]{0:T(512)S(1)} %bitcast.119, f32[259,512]{1,0:T(8,128)} %get-tuple-element.37, ...), kind=kLoop, calls=%fused_computation.105 | loop fusion | flops 3145728 | bytes 4734976
  223.9 0.3 convolution_convert_fusion.3
  224.2 0.4 copy-done.11
  224.6 0.7 pad_maximum_fusion
  225.3 0.7 mul.485
  226.0 0.6 fusion.79
  226.6 1.7 iota_compare_fusion
  228.3 2.2 convolution_convert_fusion.2
  230.5 0.2 copy.57
  230.7 0.7 slice.225
  231.4 1.5 subtract_convert_fusion
  232.9 1.3 convert_multiply_fusion
  234.2 1.3 copy.68
  235.5 3.5 %slice.232 = bf16[2048,640]{1,0:T(8,128)(2,1)} slice(bf16[2048,3712]{1,0:T(8,128)(2,1)} %all-gather.7.cloned.1.call-done), slice={[0:2048], [3072:3712]} | slice | bytes 5242880 | tf_op jit(solution)/shard_map/slice | solution.py:200
  239.0 4.5 %reshape.324 = bf16[4096,320]{1,0:T(8,128)(2,1)S(1)} reshape(bf16[2048,640]{1,0:T(8,128)(2,1)} %slice.232) | data formatting | bytes 5242880 | tf_op jit(solution)/shard_map/reshape | solution.py:200
  243.6 1.1 slice.234
  244.6 2.3 copy.61
  247.0 2.4 convolution_convert_fusion.1
  249.4 0.2 broadcast_in_dim.57
  249.7 7.9 %fusion = (f32[4,256]{1,0:T(4,128)S(1)}, f32[4,256,4096]{2,1,0:T(8,128)}) fusion(pred[256,4096]{1,0:T(8,128)(4,1)S(1)} %copy-done.4, bf16[4096,4,64]{0,2,1:T(8,128)(2,1)S(1)} %broadcast_in_dim.57, bf16[4096,4,128]{0,2,1:T(8,128)(2,1)S(1)} %bitcast.96, bf16[256,4,32]{0,2,1:T(8,128)(2,1)S(1)} %copy-done.19, bf16[256,4,32]{0,2,1:T(8,128)(2,1)S(1)} %copy-done.18, ...), kind=kOutput, calls=%fused_computation.2 | convolution fusion | flops 1636957184 | bytes 24514560 | tf_op jit(solution)/shard_map/qhd,khd->hqk/dot_general | solution.py:135
  257.6 3.3 %convolution_convert_fusion = bf16[4096,512]{0,1:T(8,128)(2,1)} fusion(bf16[256,512]{1,0:T(8,128)(2,1)S(1)} %copy-done.14, bf16[4096,320]{1,0:T(8,128)(2,1)S(1)} %reshape.324), kind=kOutput, calls=%fused_computation.14 | convolution fusion | flops 1075838976 | bytes 6553600 | tf_op jit(solution)/shard_map/dot_general | solution.py:126
  260.9 8.4 %fusion.1 = f32[4,256]{1,0:T(4,128)S(1)} fusion(f32[4,256,4096]{2,1,0:T(8,128)} %get-tuple-element.64, f32[4,256]{1,0:T(4,128)S(1)} %broadcast_maximum_fusion, pred[256,4096]{1,0:T(8,128)(4,1)S(1)} %copy-done.4), kind=kLoop, calls=%fused_computation.3 | loop fusion | flops 16776192 | bytes 17833984 | tf_op jit(solution)/shard_map/reduce_sum | solution.py:143
  269.3 2.3 copy-done.2
  271.6 6.8 %fusion.52 = bf16[256,4,128]{0,2,1:T(8,128)(2,1)S(1)} fusion(bf16[4096,4,128]{0,2,1:T(8,128)(2,1)} %bitcast.97, f32[4,256,4096]{2,1,0:T(8,128)S(1)} %copy-done.2, f32[4,256]{1,0:T(4,128)S(1)} %broadcast_maximum_fusion, pred[256,4096]{1,0:T(8,128)(4,1)S(1)} %copy-done.4, f32[256,4]{0,1:T(4,128)S(1)} %bitcast.123), kind=kOutput, calls=%fused_computation.67 | convolution fusion | flops 1090781184 | bytes 22290432 | tf_op jit(solution)/shard_map/hqk,khd->hqd/dot_general | solution.py:144
  278.4 0.8 copy.70
  279.2 0.3 fusion.67
  279.6 2.3 fusion.30
  281.9 17.9 %all-gather.9.cloned.1.call-done = bf16[16640,128]{1,0:T(8,128)(2,1)} async-done(((bf16[1040,128]{1,0:T(8,128)(2,1)}), bf16[16640,128]{1,0:T(8,128)(2,1)}) %all-gather.9.cloned.1.call-update) | async-done | bytes 4259856 | tf_op jit(solution)/shard_map/all_gather | solution.py:82
  299.8 0.8 fusion.90
  301.1 4.5 %multiply_reduce_fusion = bf16[1024,128]{1,0:T(8,128)(2,1)S(1)} fusion(bf16[16,1040,128]{2,1,0:T(8,128)(2,1)} %bitcast.102, f32[16,1024]{1,0:T(8,128)S(1)} %mul.480), kind=kLoop, calls=%fused_computation.7 | loop fusion | flops 6160384 | bytes 4521984 | tf_op jit(solution)/shard_map/reduce_sum | solution.py:93
  305.7 0.3 fusion.33
  306.0 1.0 copy-done.3
  307.3 0.3 mul.492
  307.6 1.2 copy.77
  308.8 2.6 copy.67
  311.4 2.8 multiply_convert_fusion.4
  (104 shorter events, 2.0 us)
Async XLA Ops:
  7.2 221.1 %copy-start = (bf16[2048,768]{1,0:T(8,128)(2,1)S(1)}, bf16[2048,768]{1,0:T(8,128)(2,1)}, u32[]{:S(2)}) copy-start(bf16[2048,768]{1,0:T(8,128)(2,1)} %param.26) | copy-start | bytes 9437188
  7.2 10.3 %copy-start.15 = (bf16[128,1024]{1,0:T(8,128)(2,1)S(1)}, bf16[128,1024]{1,0:T(8,128)(2,1)}, u32[]{:S(2)}) copy-start(bf16[128,1024]{1,0:T(8,128)(2,1)} %param.33) | copy-start | bytes 786436
  7.2 11.0 %copy-start.17 = (bf16[128,512]{1,0:T(8,128)(2,1)S(1)}, bf16[128,512]{1,0:T(8,128)(2,1)}, u32[]{:S(2)}) copy-start(bf16[128,512]{1,0:T(8,128)(2,1)} %param.34) | copy-start | bytes 393220
  7.2 15.4 %all-gather.5.cloned.1.call-start = ((), (), s32[]{:S(2)}) async-start(), calls=%async_computation | async-start | bytes 1572864 | tf_op jit(solution)/shard_map/all_gather | solution.py:173
  10.7 195.4 %all-gather.7.cloned.1.call-start = ((), (), s32[]{:S(2)}) async-start(), calls=%async_computation.1 | async-start | bytes 16154624 | tf_op jit(solution)/shard_map/all_gather | solution.py:197
  18.2 7.7 %copy-start.33 = (f32[256]{0:T(256)S(1)}, f32[256]{0:T(256)}, u32[]{:S(2)}) copy-start(f32[256]{0:T(256)} %fusion.81) | copy-start | bytes 3076
  18.2 7.7 %copy-start.34 = (f32[32]{0:T(128)S(1)}, f32[32]{0:T(128)}, u32[]{:S(2)}) copy-start(f32[32]{0:T(128)} %multiply_power_fusion) | copy-start | bytes 388
  20.4 9.6 %copy-start.26 = (bf16[4,512]{1,0:T(4,128)(2,1)S(1)}, bf16[4,512]{1,0:T(4,128)(2,1)}, u32[]{:S(2)}) copy-start(bf16[4,512]{1,0:T(4,128)(2,1)} %param.38) | copy-start | bytes 12292
  20.5 9.6 %copy-start.27 = (bf16[4,512]{1,0:T(4,128)(2,1)S(1)}, bf16[4,512]{1,0:T(4,128)(2,1)}, u32[]{:S(2)}) copy-start(bf16[4,512]{1,0:T(4,128)(2,1)} %param.39) | copy-start | bytes 12292
  20.5 9.6 %copy-start.25 = (bf16[4,1024]{1,0:T(4,128)(2,1)S(1)}, bf16[4,1024]{1,0:T(4,128)(2,1)}, u32[]{:S(2)}) copy-start(bf16[4,1024]{1,0:T(4,128)(2,1)} %param.37) | copy-start | bytes 24580
  28.6 271.2 %all-gather.9.cloned.1.call-start = ((), (), s32[]{:S(2)}) async-start(), calls=%async_computation.2 | async-start | bytes 4526080 | tf_op jit(solution)/shard_map/all_gather | solution.py:82
  30.8 5.5 %collective-permute-start = (bf16[8,2048]{1,0:T(8,128)(2,1)S(1)}, bf16[8,2048]{1,0:T(8,128)(2,1)S(1)}, u32[]{:S(2)}, u32[]{:S(2)}) collective-permute-start(bf16[8,2048]{1,0:T(8,128)(2,1)S(1)} %slice.235), channel_id=1, source_target_pairs={{0,2},{2,4},{4,6},{6,8},{8,10},{10,12},{12,14},{14,16},{16,18},{18... | collective-permute-start | bytes 98312 | tf_op jit(solution)/shard_map/ppermute | solution.py:19
  35.3 179.2 %copy-start.21 = (f32[4,4,256]{2,1,0:T(4,128)}, f32[4,4,256]{2,1,0:T(4,128)S(1)}, u32[]{:S(2)}) copy-start(f32[4,4,256]{2,1,0:T(4,128)S(1)} %mul.456) | copy-start | bytes 49156
  35.7 178.9 %copy-start.23 = (f32[4,4,256]{2,1,0:T(4,128)}, f32[4,4,256]{2,1,0:T(4,128)S(1)}, u32[]{:S(2)}) copy-start(f32[4,4,256]{2,1,0:T(4,128)S(1)} %fusion.68) | copy-start | bytes 49156
  214.5 1.6 copy-start.6
  217.7 7.7 %copy-start.35 = (f32[16]{0:T(128)S(1)}, f32[16]{0:T(128)}, u32[]{:S(2)}) copy-start(f32[16]{0:T(128)} %param.42) | copy-start | bytes 196
  219.7 4.2 %copy-start.9 = (bf16[256,1024]{0,1:T(8,128)(2,1)S(1)}, bf16[256,1024]{0,1:T(8,128)(2,1)}, u32[]{:S(2)}) copy-start(bf16[256,1024]{0,1:T(8,128)(2,1)} %copy.64) | copy-start | bytes 1572868
  223.9 0.7 copy-start.11
  225.3 1.3 copy-start.31
  247.0 2.4 copy-start.8
  247.0 2.7 copy-start.4
  247.0 2.7 copy-start.16
  247.0 2.7 copy-start.18
  247.0 2.7 copy-start.19
  249.7 7.9 %copy-start.14 = (bf16[256,512]{1,0:T(8,128)(2,1)S(1)}, bf16[256,512]{1,0:T(8,128)(2,1)}, u32[]{:S(2)}) copy-start(bf16[256,512]{1,0:T(8,128)(2,1)} %param.31) | copy-start | bytes 786436
  260.9 10.7 %copy-start.2 = (f32[4,256,4096]{2,1,0:T(8,128)S(1)}, f32[4,256,4096]{2,1,0:T(8,128)}, u32[]{:S(2)}) copy-start(f32[4,256,4096]{2,1,0:T(8,128)} %get-tuple-element.64) | copy-start | bytes 50331652
  271.6 7.6 %copy-start.7 = (bf16[32,4,8,128]{3,2,1,0:T(8,128)(2,1)S(1)}, bf16[32,4,8,128]{3,2,1,0:T(8,128)(2,1)}, u32[]{:S(2)}) copy-start(bf16[32,4,8,128]{3,2,1,0:T(8,128)(2,1)} %get-tuple-element.65) | copy-start | bytes 786436
  271.6 7.6 %copy-start.12 = (bf16[32,4,8,128]{3,2,1,0:T(8,128)(2,1)S(1)}, bf16[32,4,8,128]{3,2,1,0:T(8,128)(2,1)}, u32[]{:S(2)}) copy-start(bf16[32,4,8,128]{3,2,1,0:T(8,128)(2,1)} %copy-done.11) | copy-start | bytes 786436
  271.6 7.9 %copy-start.10 = (bf16[256,1024]{0,1:T(8,128)(2,1)S(1)}, bf16[256,1024]{0,1:T(8,128)(2,1)}, u32[]{:S(2)}) copy-start(bf16[256,1024]{0,1:T(8,128)(2,1)} %copy.64) | copy-start | bytes 1572868
  271.6 7.9 %copy-start.20 = (pred[256,256]{1,0:T(8,128)(4,1)S(1)}, pred[256,256]{1,0:T(8,128)(4,1)}, u32[]{:S(2)}) copy-start(pred[256,256]{1,0:T(8,128)(4,1)} %iota_compare_fusion.1) | copy-start | bytes 196612
  271.6 8.0 %copy-start.22 = (f32[4,4,256]{2,1,0:T(4,128)S(1)}, f32[4,4,256]{2,1,0:T(4,128)}, u32[]{:S(2)}) copy-start(f32[4,4,256]{2,1,0:T(4,128)} %copy-done.21) | copy-start | bytes 49156
  271.6 8.0 %copy-start.24 = (f32[4,4,256]{2,1,0:T(4,128)S(1)}, f32[4,4,256]{2,1,0:T(4,128)}, u32[]{:S(2)}) copy-start(f32[4,4,256]{2,1,0:T(4,128)} %copy-done.23) | copy-start | bytes 49156
  279.6 21.1 %copy-start.28 = (pred[16,16]{1,0:T(8,128)(4,1)S(1)}, pred[16,16]{1,0:T(8,128)(4,1)}, u32[]{:S(2)}) copy-start(pred[16,16]{1,0:T(8,128)(4,1)} %fusion.79) | copy-start | bytes 772
  279.6 21.2 %copy-start.32 = (pred[16]{0:T(512)(128)(4,1)S(1)}, pred[16]{0:T(512)(128)(4,1)}, u32[]{:S(2)}) copy-start(pred[16]{0:T(512)(128)(4,1)} %copy-done.31) | copy-start | bytes 52
  281.9 23.8 %copy-start.29 = (f32[4,4]{1,0:T(4,128)S(1)}, f32[4,4]{1,0:T(4,128)}, u32[]{:S(2)}) copy-start(f32[4,4]{1,0:T(4,128)} %mul.485) | copy-start | bytes 196
  281.9 25.1 %copy-start.5 = (f32[256,1024]{0,1:T(8,128)S(1)}, f32[256,1024]{0,1:T(8,128)}, u32[]{:S(2)}) copy-start(f32[256,1024]{0,1:T(8,128)} %copy.68) | copy-start | bytes 3145732
  301.1 4.6 %copy-start.13 = (f32[256,4,4,64]{0,3,2,1:T(8,128)S(1)}, f32[256,4,4,64]{0,3,2,1:T(8,128)}, u32[]{:S(2)}) copy-start(f32[256,4,4,64]{0,3,2,1:T(8,128)} %fusion.30) | copy-start | bytes 3145732
  306.0 1.0 copy-start.3
  307.0 4.4 %copy-start.30 = (f32[1024]{0:T(1024)S(1)}, f32[1024]{0:T(1024)}, u32[]{:S(2)}) copy-start(f32[1024]{0:T(1024)} %param.43) | copy-start | bytes 12292
  307.1 7.1 %copy-start.1 = (bf16[2048,768]{1,0:T(8,128)(2,1)S(1)}, bf16[2048,768]{1,0:T(8,128)(2,1)}, u32[]{:S(2)}) copy-start(bf16[2048,768]{1,0:T(8,128)(2,1)} %param.26) | copy-start | bytes 9437188
Sparse Core Ops, SparseCore 0:
  10.8 11.7 all-gather.4
  28.7 177.3 all-gather.6
  225.4 74.3 all-gather.8
where the time goes:
time: 322 us; the launch traced here: 321 us
  waiting for transfers between devices  190 us (59%)
  local copies, waits for them, and re-layouts  37.7 us (12%)
  matrix products  37.7 us (12%)
  other arithmetic  37.4 us (12%)
  between operations  14.3 us (4%)
  starting transfers between devices  3.75 us (1%)
    all_gather x1, waiting for transfers between devices, shards(): everything = lax.all_gather(packed, 'sp', axis=0, tiled=True)  170 us
    all_gather x1, waiting for transfers between devices, state_before(): everything = lax.all_gather(jnp.concatenate([flat, tail], axis=0), axis)  17.9 us
    unnamed x80, local copies, waits for them, and re-layouts  14.6 us
    dot_general x1, matrix products, shards(): jnp.dot(jnp.concatenate([edge_rows, rows], axis=0), everything[:, :scan_w...  8.42 us
    reduce_sum x1, other arithmetic, attend_piece(): total = jnp.sum(weights, axis=-1)  8.37 us
    dot_general x1, matrix products, attend_piece(): jnp.einsum('qhd,khd->hqk', query_whole, key_whole, preferred_element_type...  7.87 us
    dot_general x1, matrix products, attend_piece(): jnp.einsum('hqk,khd->hqd', weights.astype(jnp.bfloat16), values, preferre...  6.76 us
  transfers between devices with their start and end apart: 4, of which 3 were waited for; matrix products, arithmetic and copies ran while one was open for 21% of the time, Pallas kernels for 0%

commit v1 on v0

--- a/solution.py
+++ b/solution.py
@@ -194,7 +194,12 @@
     packed = jnp.concatenate(
         [scan_input, scan_gate, scan_write, scan_read, keys.reshape(depth, -1)], axis=1
     )
-    everything = lax.all_gather(packed, "sp", axis=0, tiled=True)
+    ring = [packed]
+    for hop in range(15):
+        ring.append(lax.ppermute(ring[-1], "sp", [(dev, (dev + 1) % 16) for dev in range(16)]))
+    everything = jnp.roll(
+        jnp.concatenate(ring[::-1], axis=0), (lax.axis_index("sp") + 1) * ring[0].shape[0], axis=0
+    )
     widths = [w.shape[1] for w in (scan_input, scan_gate, scan_write, scan_read)]
     scan_width = sum(widths)
     all_keys = everything[:, scan_width:].reshape(-1, latent_width + ROPE)

time: 322 us -> 534 us (1.66)
  waiting for transfers between devices: 190 us -> 321 us
  local copies, waits for them, and re-layouts: 37.7 us -> 102 us
  matrix products: 37.7 us -> 45.4 us
  other arithmetic: 37.4 us -> 45 us
    ppermute x0 -> x15, waiting for transfers between devices: none -> 317 us  [shards(): lax.ppermute(ring[-1], 'sp', [(dev, (dev + 1) % 16) for dev in range(16)])]
    all_gather x1 -> x0, waiting for transfers between devices: 170 us -> none  [shards(): everything = lax.all_gather(packed, 'sp', axis=0, tiled=True)]
    unnamed x80 -> x151, local copies, waits for them, and re-layouts: 14.6 us -> 64.7 us
    all_gather x1, waiting for transfers between devices: 17.9 us -> 2.48 us  [state_before(): everything = lax.all_gather(jnp.concatenate([flat, tail], axis=0), axis)]
  transfers between devices with their start and end apart: 4 -> 18, of which waited for: 3 -> 17; matrix products, arithmetic and copies ran while one was open for 21% -> 23% of each run, Pallas kernels for 0% -> 0%
where the time goes in v1:
time: 534 us; the launch traced here: 531 us
  waiting for transfers between devices  321 us (60%)
  local copies, waits for them, and re-layouts  102 us (19%)
  matrix products  45.4 us (9%)
  other arithmetic  45 us (8%)
  between operations  15 us (3%)
    ppermute x15, waiting for transfers between devices, shards(): lax.ppermute(ring[-1], 'sp', [(dev, (dev + 1) % 16) for dev in range(16)])  317 us
    unnamed x151, local copies, waits for them, and re-layouts  64.7 us
  transfers between devices with their start and end apart: 18, of which 17 were waited for; matrix products, arithmetic and copies ran while one was open for 23% of the time, Pallas kernels for 0%

profile of v1, /device:TPU:0, one launch (start us, length us, event | category | flops | bytes accessed | tf_op | source)
XLA Modules:
  0.0 531.4 jit_solution(10240252204257149498)
XLA Ops:
  7.2 1.4 fusion.40
  8.6 2.0 fusion.42
  10.7 2.0 copy.58
  12.7 1.9 copy.59
  14.6 1.7 constant_dynamic-update-slice_fusion.4
  16.3 1.7 constant_dynamic-update-slice_fusion.3
  18.0 1.6 constant_dynamic-update-slice_fusion.2
  19.6 1.6 constant_dynamic-update-slice_fusion.1
  21.2 1.4 all-gather.4.cloned.1.call-done
  22.6 3.2 fusion.24
  29.5 1.7 collective-permute-start
  31.3 25.4 %collective-permute-done = bf16[128,3712]{1,0:T(8,128)(2,1)S(1)} collective-permute-done((bf16[128,3712]{1,0:T(8,128)(2,1)}, bf16[128,3712]{1,0:T(8,128)(2,1)S(1)}, u32[]{:S(2)}, u32[]{:S(2)}) %collective-permute-start) | collective-permute-done | bytes 950304 | tf_op jit(solution)/shard_map/ppermute | solution.py:199
  57.6 26.1 %collective-permute-done.1 = bf16[128,3712]{1,0:T(8,128)(2,1)S(1)} collective-permute-done((bf16[128,3712]{1,0:T(8,128)(2,1)S(1)}, bf16[128,3712]{1,0:T(8,128)(2,1)S(1)}, u32[]{:S(2)}, u32[]{:S(2)}) %collective-permute-start.1) | collective-permute-done | bytes 950304 | tf_op jit(solution)/shard_map/ppermute | solution.py:199
  84.7 25.2 %collective-permute-done.2 = bf16[128,3712]{1,0:T(8,128)(2,1)S(1)} collective-permute-done((bf16[128,3712]{1,0:T(8,128)(2,1)S(1)}, bf16[128,3712]{1,0:T(8,128)(2,1)S(1)}, u32[]{:S(2)}, u32[]{:S(2)}) %collective-permute-start.2) | collective-permute-done | bytes 950304 | tf_op jit(solution)/shard_map/ppermute | solution.py:199
  110.8 24.3 %collective-permute-done.3 = bf16[128,3712]{1,0:T(8,128)(2,1)S(1)} collective-permute-done((bf16[128,3712]{1,0:T(8,128)(2,1)S(1)}, bf16[128,3712]{1,0:T(8,128)(2,1)S(1)}, u32[]{:S(2)}, u32[]{:S(2)}) %collective-permute-start.3) | collective-permute-done | bytes 950304 | tf_op jit(solution)/shard_map/ppermute | solution.py:199
  136.1 23.5 %collective-permute-done.4 = bf16[128,3712]{1,0:T(8,128)(2,1)S(1)} collective-permute-done((bf16[128,3712]{1,0:T(8,128)(2,1)S(1)}, bf16[128,3712]{1,0:T(8,128)(2,1)S(1)}, u32[]{:S(2)}, u32[]{:S(2)}) %collective-permute-start.4) | collective-permute-done | bytes 950304 | tf_op jit(solution)/shard_map/ppermute | solution.py:199
  160.6 22.6 %collective-permute-done.5 = bf16[128,3712]{1,0:T(8,128)(2,1)S(1)} collective-permute-done((bf16[128,3712]{1,0:T(8,128)(2,1)S(1)}, bf16[128,3712]{1,0:T(8,128)(2,1)S(1)}, u32[]{:S(2)}, u32[]{:S(2)}) %collective-permute-start.5) | collective-permute-done | bytes 950304 | tf_op jit(solution)/shard_map/ppermute | solution.py:199
  184.2 21.8 %collective-permute-done.6 = bf16[128,3712]{1,0:T(8,128)(2,1)S(1)} collective-permute-done((bf16[128,3712]{1,0:T(8,128)(2,1)S(1)}, bf16[128,3712]{1,0:T(8,128)(2,1)S(1)}, u32[]{:S(2)}, u32[]{:S(2)}) %collective-permute-start.6) | collective-permute-done | bytes 950304 | tf_op jit(solution)/shard_map/ppermute | solution.py:199
  206.9 20.9 %collective-permute-done.7 = bf16[128,3712]{1,0:T(8,128)(2,1)S(1)} collective-permute-done((bf16[128,3712]{1,0:T(8,128)(2,1)S(1)}, bf16[128,3712]{1,0:T(8,128)(2,1)S(1)}, u32[]{:S(2)}, u32[]{:S(2)}) %collective-permute-start.7) | collective-permute-done | bytes 950304 | tf_op jit(solution)/shard_map/ppermute | solution.py:199
  228.8 20.2 %collective-permute-done.8 = bf16[128,3712]{1,0:T(8,128)(2,1)S(1)} collective-permute-done((bf16[128,3712]{1,0:T(8,128)(2,1)S(1)}, bf16[128,3712]{1,0:T(8,128)(2,1)S(1)}, u32[]{:S(2)}, u32[]{:S(2)}) %collective-permute-start.8) | collective-permute-done | bytes 950304 | tf_op jit(solution)/shard_map/ppermute | solution.py:199
  250.0 20.3 %collective-permute-done.9 = bf16[128,3712]{1,0:T(8,128)(2,1)S(1)} collective-permute-done((bf16[128,3712]{1,0:T(8,128)(2,1)S(1)}, bf16[128,3712]{1,0:T(8,128)(2,1)S(1)}, u32[]{:S(2)}, u32[]{:S(2)}) %collective-permute-start.9) | collective-permute-done | bytes 950304 | tf_op jit(solution)/shard_map/ppermute | solution.py:199
  271.2 20.3 %collective-permute-done.10 = bf16[128,3712]{1,0:T(8,128)(2,1)S(1)} collective-permute-done((bf16[128,3712]{1,0:T(8,128)(2,1)S(1)}, bf16[128,3712]{1,0:T(8,128)(2,1)S(1)}, u32[]{:S(2)}, u32[]{:S(2)}) %collective-permute-start.10) | collective-permute-done | bytes 950304 | tf_op jit(solution)/shard_map/ppermute | solution.py:199
  292.4 20.3 %collective-permute-done.11 = bf16[128,3712]{1,0:T(8,128)(2,1)S(1)} collective-permute-done((bf16[128,3712]{1,0:T(8,128)(2,1)S(1)}, bf16[128,3712]{1,0:T(8,128)(2,1)S(1)}, u32[]{:S(2)}, u32[]{:S(2)}) %collective-permute-start.11) | collective-permute-done | bytes 950304 | tf_op jit(solution)/shard_map/ppermute | solution.py:199
  314.3 21.3 %collective-permute-done.12 = bf16[128,3712]{1,0:T(8,128)(2,1)} collective-permute-done((bf16[128,3712]{1,0:T(8,128)(2,1)S(1)}, bf16[128,3712]{1,0:T(8,128)(2,1)}, u32[]{:S(2)}, u32[]{:S(2)}) %collective-permute-start.12) | collective-permute-done | bytes 950304 | tf_op jit(solution)/shard_map/ppermute | solution.py:199
  336.9 1.5 slice_convert_fusion.11
  338.3 1.4 slice_convert_fusion.15
  339.8 1.5 slice_convert_fusion.7
  341.2 1.4 slice.234
  342.6 1.9 collective-permute-start.15
  344.5 14.5 %collective-permute-done.13 = bf16[128,3712]{1,0:T(8,128)(2,1)} collective-permute-done((bf16[128,3712]{1,0:T(8,128)(2,1)}, bf16[128,3712]{1,0:T(8,128)(2,1)}, u32[]{:S(2)}, u32[]{:S(2)}) %collective-permute-start.13) | collective-permute-done | bytes 950304 | tf_op jit(solution)/shard_map/ppermute | solution.py:199
  358.9 1.4 add_bitcast_fusion
  360.3 1.3 reshape.330
  365.0 1.5 exponential_bitcast_fusion
  366.5 10.1 %collective-permute-done.14 = bf16[128,3712]{1,0:T(8,128)(2,1)} collective-permute-done((bf16[128,3712]{1,0:T(8,128)(2,1)}, bf16[128,3712]{1,0:T(8,128)(2,1)}, u32[]{:S(2)}, u32[]{:S(2)}) %collective-permute-start.14) | collective-permute-done | bytes 950304 | tf_op jit(solution)/shard_map/ppermute | solution.py:199
  404.8 10.0 %copy-done.34 = bf16[4096,3712]{1,0:T(8,128)(2,1)} copy-done((bf16[4096,3712]{1,0:T(8,128)(2,1)}, bf16[4096,3712]{1,0:T(8,128)(2,1)S(1)}, u32[]{:S(2)}) %copy-start.34) | copy-done | bytes 30408728
  414.9 8.1 %fusion.12 = bf16[264,3072]{1,0:T(8,128)(2,1)S(1)} fusion(bf16[4096,3712]{1,0:T(8,128)(2,1)} %copy-done.34, s32[]{:T(128)S(6)} %select_n.47, bf16[256,2048]{1,0:T(8,128)(2,1)S(1)} %copy-done.51, bf16[8,2048]{1,0:T(8,128)(2,1)} %collective-permute-done.15), kind=kOutput, calls=%fused_computation.18 | convolution fusion | flops 3324862464 | bytes 15286276 | tf_op jit(solution)/shard_map/dot_general | solution.py:206
  424.6 1.4 multiply_convert_fusion.6
  426.1 2.1 copy.64
  428.1 3.1 fusion.71
  432.0 1.3 convolution_convert_fusion.3
  433.3 1.4 pad_maximum_fusion
  434.8 1.3 mul.489
  436.7 2.3 iota_compare_fusion
  439.0 3.0 convolution_convert_fusion.2
  442.0 1.9 copy.57
  443.9 1.7 slice.225
  447.2 2.3 convert_multiply_fusion
  449.6 2.5 copy.68
  452.1 3.5 dynamic-slice.15
  455.6 5.8 %reshape.324 = bf16[4096,320]{1,0:T(8,128)(2,1)} reshape(bf16[2048,640]{1,0:T(8,128)(2,1)} %dynamic-slice.15) | data formatting | bytes 5242880 | tf_op jit(solution)/shard_map/reshape | solution.py:205
  461.4 2.3 slice.233
  463.7 2.3 copy.61
  466.1 3.0 convolution_convert_fusion.1
  470.4 9.2 %fusion = (f32[4,256]{1,0:T(4,128)S(1)}, f32[4,256,4096]{2,1,0:T(8,128)}) fusion(pred[256,4096]{1,0:T(8,128)(4,1)} %iota_compare_fusion, bf16[4096,4,64]{0,2,1:T(8,128)(2,1)S(1)} %broadcast_in_dim.57, bf16[4096,4,128]{0,2,1:T(8,128)(2,1)S(1)} %bitcast.96, bf16[256,4,32]{0,2,1:T(8,128)(2,1)S(1)} %copy-done.37, bf16[256,4,32]{0,2,1:T(8,128)(2,1)S(1)} %copy-done.36, ...), kind=kOutput, calls=%fused_computation.2 | convolution fusion | flops 1636957184 | bytes 24514560 | tf_op jit(solution)/shard_map/qhd,khd->hqk/dot_general | solution.py:135
  480.9 8.1 %fusion.1 = f32[4,256]{1,0:T(4,128)S(1)} fusion(f32[4,256,4096]{2,1,0:T(8,128)} %get-tuple-element.64, f32[4,256]{1,0:T(4,128)S(1)} %broadcast_maximum_fusion, pred[256,4096]{1,0:T(8,128)(4,1)S(1)} %copy-done.3), kind=kLoop, calls=%fused_computation.3 | loop fusion | flops 16776192 | bytes 17833984 | tf_op jit(solution)/shard_map/reduce_sum | solution.py:143
  489.1 8.9 %fusion.52 = bf16[256,4,128]{0,2,1:T(8,128)(2,1)} fusion(bf16[4096,4,128]{0,2,1:T(8,128)(2,1)S(1)} %bitcast.97, f32[4,256,4096]{2,1,0:T(8,128)} %get-tuple-element.64, f32[4,256]{1,0:T(4,128)S(1)} %broadcast_maximum_fusion, pred[256,4096]{1,0:T(8,128)(4,1)S(1)} %copy-done.3, f32[256,4]{0,1:T(4,128)S(1)} %bitcast.123), kind=kOutput, calls=%fused_computation.67 | convolution fusion | flops 1090781184 | bytes 22290432 | tf_op jit(solution)/shard_map/hqk,khd->hqd/dot_general | solution.py:144
  498.0 1.8 copy.70
  501.0 3.4 fusion.30
  504.5 2.5 all-gather.6.cloned.1.call-done
  508.9 4.5 multiply_reduce_fusion
  513.3 1.7 fusion.33
  516.0 1.4 multiply_reduce_fusion.1
  519.1 2.5 copy.67
  521.7 2.9 multiply_convert_fusion.4
  (203 shorter events, 61.3 us)
Async XLA Ops:
  7.2 431.9 %copy-start = (bf16[2048,768]{1,0:T(8,128)(2,1)S(1)}, bf16[2048,768]{1,0:T(8,128)(2,1)}, u32[]{:S(2)}) copy-start(bf16[2048,768]{1,0:T(8,128)(2,1)} %param.26) | copy-start | bytes 9437188
  7.2 390.9 %copy-start.31 = (bf16[128,512]{1,0:T(8,128)(2,1)S(1)}, bf16[128,512]{1,0:T(8,128)(2,1)}, u32[]{:S(2)}) copy-start(bf16[128,512]{1,0:T(8,128)(2,1)} %param.34) | copy-start | bytes 393220
  7.2 15.4 %all-gather.4.cloned.1.call-start = ((), (), s32[]{:S(2)}) async-start(), calls=%async_computation | async-start | bytes 1572864 | tf_op jit(solution)/shard_map/all_gather | solution.py:173
  10.7 496.3 %all-gather.6.cloned.1.call-start = ((), (), s32[]{:S(2)}) async-start(), calls=%async_computation.1 | async-start | bytes 4526080 | tf_op jit(solution)/shard_map/all_gather | solution.py:82
  29.5 27.1 %collective-permute-start = (bf16[128,3712]{1,0:T(8,128)(2,1)}, bf16[128,3712]{1,0:T(8,128)(2,1)S(1)}, u32[]{:S(2)}, u32[]{:S(2)}) collective-permute-start(bf16[128,3712]{1,0:T(8,128)(2,1)} %constant_dynamic-update-slice_fusion), channel_id=1, source_target_pairs={{0,2},{2,4},{4,6},{6,8},{8,10},{10,12},{12,14},{14,16},{16,18},{18... | collective-permute-start | bytes 2850824 | tf_op jit(solution)/shard_map/ppermute | solution.py:199
  56.7 1.0 copy-start.4
  57.6 26.1 %collective-permute-start.1 = (bf16[128,3712]{1,0:T(8,128)(2,1)S(1)}, bf16[128,3712]{1,0:T(8,128)(2,1)S(1)}, u32[]{:S(2)}, u32[]{:S(2)}) collective-permute-start(bf16[128,3712]{1,0:T(8,128)(2,1)S(1)} %collective-permute-done), channel_id=1, source_target_pairs={{0,2},{2,4},{4,6},{6,8},{8,10},{10,12},{12,14},{14,16},{16,18},{18... | collective-permute-start | bytes 2850824 | tf_op jit(solution)/shard_map/ppermute | solution.py:199
  83.7 1.0 copy-start.6
  84.6 25.2 %collective-permute-start.2 = (bf16[128,3712]{1,0:T(8,128)(2,1)S(1)}, bf16[128,3712]{1,0:T(8,128)(2,1)S(1)}, u32[]{:S(2)}, u32[]{:S(2)}) collective-permute-start(bf16[128,3712]{1,0:T(8,128)(2,1)S(1)} %collective-permute-done.1), channel_id=1, source_target_pairs={{0,2},{2,4},{4,6},{6,8},{8,10},{10,12},{12,14},{14,16},{16,18},{18... | collective-permute-start | bytes 2850824 | tf_op jit(solution)/shard_map/ppermute | solution.py:199
  109.9 0.9 copy-start.8
  110.8 24.3 %collective-permute-start.3 = (bf16[128,3712]{1,0:T(8,128)(2,1)S(1)}, bf16[128,3712]{1,0:T(8,128)(2,1)S(1)}, u32[]{:S(2)}, u32[]{:S(2)}) collective-permute-start(bf16[128,3712]{1,0:T(8,128)(2,1)S(1)} %collective-permute-done.2), channel_id=1, source_target_pairs={{0,2},{2,4},{4,6},{6,8},{8,10},{10,12},{12,14},{14,16},{16,18},{18... | collective-permute-start | bytes 2850824 | tf_op jit(solution)/shard_map/ppermute | solution.py:199
  135.1 0.9 copy-start.10
  136.1 23.5 %collective-permute-start.4 = (bf16[128,3712]{1,0:T(8,128)(2,1)S(1)}, bf16[128,3712]{1,0:T(8,128)(2,1)S(1)}, u32[]{:S(2)}, u32[]{:S(2)}) collective-permute-start(bf16[128,3712]{1,0:T(8,128)(2,1)S(1)} %collective-permute-done.3), channel_id=1, source_target_pairs={{0,2},{2,4},{4,6},{6,8},{8,10},{10,12},{12,14},{14,16},{16,18},{18... | collective-permute-start | bytes 2850824 | tf_op jit(solution)/shard_map/ppermute | solution.py:199
  159.6 1.0 copy-start.12
  160.6 22.6 %collective-permute-start.5 = (bf16[128,3712]{1,0:T(8,128)(2,1)S(1)}, bf16[128,3712]{1,0:T(8,128)(2,1)S(1)}, u32[]{:S(2)}, u32[]{:S(2)}) collective-permute-start(bf16[128,3712]{1,0:T(8,128)(2,1)S(1)} %collective-permute-done.4), channel_id=1, source_target_pairs={{0,2},{2,4},{4,6},{6,8},{8,10},{10,12},{12,14},{14,16},{16,18},{18... | collective-permute-start | bytes 2850824 | tf_op jit(solution)/shard_map/ppermute | solution.py:199
  183.2 1.0 copy-start.14
  184.2 21.8 %collective-permute-start.6 = (bf16[128,3712]{1,0:T(8,128)(2,1)S(1)}, bf16[128,3712]{1,0:T(8,128)(2,1)S(1)}, u32[]{:S(2)}, u32[]{:S(2)}) collective-permute-start(bf16[128,3712]{1,0:T(8,128)(2,1)S(1)} %collective-permute-done.5), channel_id=1, source_target_pairs={{0,2},{2,4},{4,6},{6,8},{8,10},{10,12},{12,14},{14,16},{16,18},{18... | collective-permute-start | bytes 2850824 | tf_op jit(solution)/shard_map/ppermute | solution.py:199
  206.9 20.9 %collective-permute-start.7 = (bf16[128,3712]{1,0:T(8,128)(2,1)S(1)}, bf16[128,3712]{1,0:T(8,128)(2,1)S(1)}, u32[]{:S(2)}, u32[]{:S(2)}) collective-permute-start(bf16[128,3712]{1,0:T(8,128)(2,1)S(1)} %collective-permute-done.6), channel_id=1, source_target_pairs={{0,2},{2,4},{4,6},{6,8},{8,10},{10,12},{12,14},{14,16},{16,18},{18... | collective-permute-start | bytes 2850824 | tf_op jit(solution)/shard_map/ppermute | solution.py:199
  227.8 1.0 copy-start.18
  228.8 20.2 %collective-permute-start.8 = (bf16[128,3712]{1,0:T(8,128)(2,1)S(1)}, bf16[128,3712]{1,0:T(8,128)(2,1)S(1)}, u32[]{:S(2)}, u32[]{:S(2)}) collective-permute-start(bf16[128,3712]{1,0:T(8,128)(2,1)S(1)} %collective-permute-done.7), channel_id=1, source_target_pairs={{0,2},{2,4},{4,6},{6,8},{8,10},{10,12},{12,14},{14,16},{16,18},{18... | collective-permute-start | bytes 2850824 | tf_op jit(solution)/shard_map/ppermute | solution.py:199
  249.0 1.0 copy-start.20
  250.0 20.3 %collective-permute-start.9 = (bf16[128,3712]{1,0:T(8,128)(2,1)S(1)}, bf16[128,3712]{1,0:T(8,128)(2,1)S(1)}, u32[]{:S(2)}, u32[]{:S(2)}) collective-permute-start(bf16[128,3712]{1,0:T(8,128)(2,1)S(1)} %collective-permute-done.8), channel_id=1, source_target_pairs={{0,2},{2,4},{4,6},{6,8},{8,10},{10,12},{12,14},{14,16},{16,18},{18... | collective-permute-start | bytes 2850824 | tf_op jit(solution)/shard_map/ppermute | solution.py:199
  271.2 20.3 %collective-permute-start.10 = (bf16[128,3712]{1,0:T(8,128)(2,1)S(1)}, bf16[128,3712]{1,0:T(8,128)(2,1)S(1)}, u32[]{:S(2)}, u32[]{:S(2)}) collective-permute-start(bf16[128,3712]{1,0:T(8,128)(2,1)S(1)} %collective-permute-done.9), channel_id=1, source_target_pairs={{0,2},{2,4},{4,6},{6,8},{8,10},{10,12},{12,14},{14,16},{16,18},{18... | collective-permute-start | bytes 2850824 | tf_op jit(solution)/shard_map/ppermute | solution.py:199
  292.4 20.3 %collective-permute-start.11 = (bf16[128,3712]{1,0:T(8,128)(2,1)S(1)}, bf16[128,3712]{1,0:T(8,128)(2,1)S(1)}, u32[]{:S(2)}, u32[]{:S(2)}) collective-permute-start(bf16[128,3712]{1,0:T(8,128)(2,1)S(1)} %collective-permute-done.10), channel_id=1, source_target_pairs={{0,2},{2,4},{4,6},{6,8},{8,10},{10,12},{12,14},{14,16},{16,18},{18... | collective-permute-start | bytes 2850824 | tf_op jit(solution)/shard_map/ppermute | solution.py:199
  313.6 22.0 %collective-permute-start.12 = (bf16[128,3712]{1,0:T(8,128)(2,1)S(1)}, bf16[128,3712]{1,0:T(8,128)(2,1)}, u32[]{:S(2)}, u32[]{:S(2)}) collective-permute-start(bf16[128,3712]{1,0:T(8,128)(2,1)S(1)} %collective-permute-done.11), channel_id=1, source_target_pairs={{0,2},{2,4},{4,6},{6,8},{8,10},{10,12},{12,14},{14,16},{16,18},{18... | collective-permute-start | bytes 2850824 | tf_op jit(solution)/shard_map/ppermute | solution.py:199
  335.6 23.3 %collective-permute-start.13 = (bf16[128,3712]{1,0:T(8,128)(2,1)}, bf16[128,3712]{1,0:T(8,128)(2,1)}, u32[]{:S(2)}, u32[]{:S(2)}) collective-permute-start(bf16[128,3712]{1,0:T(8,128)(2,1)} %collective-permute-done.12), channel_id=1, source_target_pairs={{0,2},{2,4},{4,6},{6,8},{8,10},{10,12},{12,14},{14,16},{16,18},{18... | collective-permute-start | bytes 2850824 | tf_op jit(solution)/shard_map/ppermute | solution.py:199
  342.6 72.2 %collective-permute-start.15 = (bf16[8,2048]{1,0:T(8,128)(2,1)}, bf16[8,2048]{1,0:T(8,128)(2,1)}, u32[]{:S(2)}, u32[]{:S(2)}) collective-permute-start(bf16[8,2048]{1,0:T(8,128)(2,1)} %slice.234), channel_id=1, source_target_pairs={{0,2},{2,4},{4,6},{6,8},{8,10},{10,12},{12,14},{14,16},{16,18},{18... | collective-permute-start | bytes 98312 | tf_op jit(solution)/shard_map/ppermute | solution.py:19
  358.9 17.7 %collective-permute-start.14 = (bf16[128,3712]{1,0:T(8,128)(2,1)}, bf16[128,3712]{1,0:T(8,128)(2,1)}, u32[]{:S(2)}, u32[]{:S(2)}) collective-permute-start(bf16[128,3712]{1,0:T(8,128)(2,1)} %collective-permute-done.13), channel_id=1, source_target_pairs={{0,2},{2,4},{4,6},{6,8},{8,10},{10,12},{12,14},{14,16},{16,18},{18... | collective-permute-start | bytes 2850824 | tf_op jit(solution)/shard_map/ppermute | solution.py:199
  361.7 43.1 %copy-start.39 = (f32[4,4,256]{2,1,0:T(4,128)}, f32[4,4,256]{2,1,0:T(4,128)S(1)}, u32[]{:S(2)}) copy-start(f32[4,4,256]{2,1,0:T(4,128)S(1)} %mul.460) | copy-start | bytes 49156
  362.7 42.1 %copy-start.41 = (f32[4,4,256]{2,1,0:T(4,128)}, f32[4,4,256]{2,1,0:T(4,128)S(1)}, u32[]{:S(2)}) copy-start(f32[4,4,256]{2,1,0:T(4,128)S(1)} %fusion.68) | copy-start | bytes 49156
  364.9 38.1 %copy-start.27 = (bf16[128,3712]{1,0:T(8,128)(2,1)S(1)}, bf16[128,3712]{1,0:T(8,128)(2,1)}, u32[]{:S(2)}) copy-start(bf16[128,3712]{1,0:T(8,128)(2,1)} %copy-done.26) | copy-start | bytes 2850820
  364.9 38.3 %copy-start.25 = (bf16[128,3712]{1,0:T(8,128)(2,1)S(1)}, bf16[128,3712]{1,0:T(8,128)(2,1)}, u32[]{:S(2)}) copy-start(bf16[128,3712]{1,0:T(8,128)(2,1)} %copy-done.24) | copy-start | bytes 2850820
  364.9 38.4 %copy-start.23 = (bf16[128,3712]{1,0:T(8,128)(2,1)S(1)}, bf16[128,3712]{1,0:T(8,128)(2,1)}, u32[]{:S(2)}) copy-start(bf16[128,3712]{1,0:T(8,128)(2,1)} %copy-done.22) | copy-start | bytes 2850820
  364.9 38.5 %copy-start.21 = (bf16[128,3712]{1,0:T(8,128)(2,1)S(1)}, bf16[128,3712]{1,0:T(8,128)(2,1)}, u32[]{:S(2)}) copy-start(bf16[128,3712]{1,0:T(8,128)(2,1)} %copy-done.20) | copy-start | bytes 2850820
  364.9 38.6 %copy-start.19 = (bf16[128,3712]{1,0:T(8,128)(2,1)S(1)}, bf16[128,3712]{1,0:T(8,128)(2,1)}, u32[]{:S(2)}) copy-start(bf16[128,3712]{1,0:T(8,128)(2,1)} %copy-done.18) | copy-start | bytes 2850820
  364.9 38.8 %copy-start.17 = (bf16[128,3712]{1,0:T(8,128)(2,1)S(1)}, bf16[128,3712]{1,0:T(8,128)(2,1)}, u32[]{:S(2)}) copy-start(bf16[128,3712]{1,0:T(8,128)(2,1)} %copy-done.16) | copy-start | bytes 2850820
  364.9 38.9 %copy-start.15 = (bf16[128,3712]{1,0:T(8,128)(2,1)S(1)}, bf16[128,3712]{1,0:T(8,128)(2,1)}, u32[]{:S(2)}) copy-start(bf16[128,3712]{1,0:T(8,128)(2,1)} %copy-done.14) | copy-start | bytes 2850820
  364.9 39.0 %copy-start.13 = (bf16[128,3712]{1,0:T(8,128)(2,1)S(1)}, bf16[128,3712]{1,0:T(8,128)(2,1)}, u32[]{:S(2)}) copy-start(bf16[128,3712]{1,0:T(8,128)(2,1)} %copy-done.12) | copy-start | bytes 2850820
  364.9 39.2 %copy-start.11 = (bf16[128,3712]{1,0:T(8,128)(2,1)S(1)}, bf16[128,3712]{1,0:T(8,128)(2,1)}, u32[]{:S(2)}) copy-start(bf16[128,3712]{1,0:T(8,128)(2,1)} %copy-done.10) | copy-start | bytes 2850820
  365.0 39.3 %copy-start.9 = (bf16[128,3712]{1,0:T(8,128)(2,1)S(1)}, bf16[128,3712]{1,0:T(8,128)(2,1)}, u32[]{:S(2)}) copy-start(bf16[128,3712]{1,0:T(8,128)(2,1)} %copy-done.8) | copy-start | bytes 2850820
  365.0 39.4 %copy-start.7 = (bf16[128,3712]{1,0:T(8,128)(2,1)S(1)}, bf16[128,3712]{1,0:T(8,128)(2,1)}, u32[]{:S(2)}) copy-start(bf16[128,3712]{1,0:T(8,128)(2,1)} %copy-done.6) | copy-start | bytes 2850820
  365.0 39.5 %copy-start.5 = (bf16[128,3712]{1,0:T(8,128)(2,1)S(1)}, bf16[128,3712]{1,0:T(8,128)(2,1)}, u32[]{:S(2)}) copy-start(bf16[128,3712]{1,0:T(8,128)(2,1)} %copy-done.4) | copy-start | bytes 2850820
  365.0 39.7 %copy-start.29 = (bf16[128,1024]{1,0:T(8,128)(2,1)S(1)}, bf16[128,1024]{1,0:T(8,128)(2,1)}, u32[]{:S(2)}) copy-start(bf16[128,1024]{1,0:T(8,128)(2,1)} %param.32) | copy-start | bytes 786436
  365.0 39.7 %copy-start.30 = (bf16[128,1024]{1,0:T(8,128)(2,1)S(1)}, bf16[128,1024]{1,0:T(8,128)(2,1)}, u32[]{:S(2)}) copy-start(bf16[128,1024]{1,0:T(8,128)(2,1)} %param.33) | copy-start | bytes 786436
  365.0 39.7 %copy-start.32 = (bf16[128,512]{1,0:T(8,128)(2,1)S(1)}, bf16[128,512]{1,0:T(8,128)(2,1)}, u32[]{:S(2)}) copy-start(bf16[128,512]{1,0:T(8,128)(2,1)} %param.35) | copy-start | bytes 393220
  366.5 48.3 %copy-start.51 = (bf16[256,2048]{1,0:T(8,128)(2,1)S(1)}, bf16[256,2048]{1,0:T(8,128)(2,1)}, u32[]{:S(2)}) copy-start(bf16[256,2048]{1,0:T(8,128)(2,1)} %all-gather.4.cloned.1.call-done) | copy-start | bytes 3145732
  403.7 20.9 %copy-start.44 = (f32[1,1024]{1,0:T(1,128)S(1)}, f32[1,1024]{1,0:T(1,128)}, u32[]{:S(2)}) copy-start(f32[1,1024]{1,0:T(1,128)} %get-tuple-element.47) | copy-start | bytes 12292
  403.7 20.9 %copy-start.45 = (f32[1,1024]{1,0:T(1,128)S(1)}, f32[1,1024]{1,0:T(1,128)}, u32[]{:S(2)}) copy-start(f32[1,1024]{1,0:T(1,128)} %get-tuple-element.48) | copy-start | bytes 12292
  403.7 20.9 %copy-start.46 = (f32[1,1024]{1,0:T(1,128)S(1)}, f32[1,1024]{1,0:T(1,128)}, u32[]{:S(2)}) copy-start(f32[1,1024]{1,0:T(1,128)} %get-tuple-element.49) | copy-start | bytes 12292
  403.7 20.9 %copy-start.47 = (f32[1,1024]{1,0:T(1,128)S(1)}, f32[1,1024]{1,0:T(1,128)}, u32[]{:S(2)}) copy-start(f32[1,1024]{1,0:T(1,128)} %get-tuple-element.50) | copy-start | bytes 12292
  404.8 10.0 %copy-start.34 = (bf16[4096,3712]{1,0:T(8,128)(2,1)}, bf16[4096,3712]{1,0:T(8,128)(2,1)S(1)}, u32[]{:S(2)}) copy-start(bf16[4096,3712]{1,0:T(8,128)(2,1)S(1)} %constant_dynamic-update-slice_fusion.37) | copy-start | bytes 91226112
  423.0 1.5 copy-start.28
  434.7 11.8 %copy-start.49 = (pred[16]{0:T(512)(128)(4,1)}, pred[16]{0:T(512)(128)(4,1)S(1)}, u32[]{:S(2)}) copy-start(pred[16]{0:T(512)(128)(4,1)S(1)} %iota_compare_fusion.4) | copy-start | bytes 52
  447.2 23.2 %copy-start.36 = (bf16[256,4,32]{0,2,1:T(8,128)(2,1)S(1)}, bf16[256,4,32]{0,2,1:T(8,128)(2,1)}, u32[]{:S(2)}) copy-start(bf16[256,4,32]{0,2,1:T(8,128)(2,1)} %get-tuple-element.41) | copy-start | bytes 196612
  447.2 23.2 %copy-start.37 = (bf16[256,4,32]{0,2,1:T(8,128)(2,1)S(1)}, bf16[256,4,32]{0,2,1:T(8,128)(2,1)}, u32[]{:S(2)}) copy-start(bf16[256,4,32]{0,2,1:T(8,128)(2,1)} %get-tuple-element.42) | copy-start | bytes 196612
  466.0 13.5 %copy-start.1 = (bf16[4096,320]{1,0:T(8,128)(2,1)S(1)}, bf16[4096,320]{1,0:T(8,128)(2,1)}, u32[]{:S(2)}) copy-start(bf16[4096,320]{1,0:T(8,128)(2,1)} %reshape.324) | copy-start | bytes 7864324
  466.1 13.5 %copy-start.35 = (bf16[256,512]{1,0:T(8,128)(2,1)S(1)}, bf16[256,512]{1,0:T(8,128)(2,1)}, u32[]{:S(2)}) copy-start(bf16[256,512]{1,0:T(8,128)(2,1)} %param.31) | copy-start | bytes 786436
  466.1 14.8 %copy-start.3 = (pred[256,4096]{1,0:T(8,128)(4,1)S(1)}, pred[256,4096]{1,0:T(8,128)(4,1)}, u32[]{:S(2)}) copy-start(pred[256,4096]{1,0:T(8,128)(4,1)} %iota_compare_fusion) | copy-start | bytes 3145732
  489.0 12.0 %copy-start.38 = (pred[256,256]{1,0:T(8,128)(4,1)S(1)}, pred[256,256]{1,0:T(8,128)(4,1)}, u32[]{:S(2)}) copy-start(pred[256,256]{1,0:T(8,128)(4,1)} %iota_compare_fusion.1) | copy-start | bytes 196612
  489.0 12.0 %copy-start.40 = (f32[4,4,256]{2,1,0:T(4,128)S(1)}, f32[4,4,256]{2,1,0:T(4,128)}, u32[]{:S(2)}) copy-start(f32[4,4,256]{2,1,0:T(4,128)} %copy-done.39) | copy-start | bytes 49156
  489.1 12.0 %copy-start.42 = (f32[4,4,256]{2,1,0:T(4,128)S(1)}, f32[4,4,256]{2,1,0:T(4,128)}, u32[]{:S(2)}) copy-start(f32[4,4,256]{2,1,0:T(4,128)} %copy-done.41) | copy-start | bytes 49156
  489.1 18.8 %copy-start.48 = (pred[16,16]{1,0:T(8,128)(4,1)S(1)}, pred[16,16]{1,0:T(8,128)(4,1)}, u32[]{:S(2)}) copy-start(pred[16,16]{1,0:T(8,128)(4,1)} %fusion.79) | copy-start | bytes 772
  489.1 18.9 %copy-start.50 = (pred[16]{0:T(512)(128)(4,1)S(1)}, pred[16]{0:T(512)(128)(4,1)}, u32[]{:S(2)}) copy-start(pred[16]{0:T(512)(128)(4,1)} %copy-done.49) | copy-start | bytes 52
  515.0 1.0 copy-start.2
  (6 other events, 5.1 us)
Sparse Core Ops, SparseCore 0:
  10.8 11.7 all-gather.3
  434.9 72.0 all-gather.5
